TPU v7x, 32 devices: a whole 2x2x4 slice. The times are simulated.
32 devices in a mesh: sp: 4 (over y, x), tp: 8 (over z, core).
Axes of the slice: x: 2, y: 2, z: 4, core: 2. Of those that a mesh axis runs over, the one named last changes fastest.
Arguments:
- moe_input: bfloat16 [512, 2048], P('sp'), may hold values from -6 to 6
- cotangent: bfloat16 [512, 2048], P('sp'), may hold values from -6 to 6
- route_expert: int32 [512, 2], P('sp'), may hold values from 0 to 3, all different within a row; in each aligned block of 128 rows (0 to 127, 128 to 255, ...) at most 128 rows name the same one
- route_weight: float32 [512, 2], P('sp'), may hold values from 0.2 to 1
- w_gate: bfloat16 [4, 2048, 6144], P('sp', None, 'tp'), may hold values from -0.125 to 0.125
- w_up: bfloat16 [4, 2048, 6144], P('sp', None, 'tp'), may hold values from -0.125 to 0.125
- w_down: bfloat16 [4, 6144, 2048], P('sp', 'tp'), may hold values from -0.078125 to 0.078125
- out_proj: bfloat16 [2048, 2048], P('tp'), may hold values from -0.125 to 0.125
- saved_out: bfloat16 [512, 2048], P('sp', 'tp'), may hold values from -6 to 6
- queries: bfloat16 [512, 1024], P('sp', 'tp'), may hold values from -6 to 6
- keys: bfloat16 [512, 1024], P('sp', 'tp'), may hold values from -6 to 6
- values: bfloat16 [512, 2048], P('sp', 'tp'), may hold values from -6 to 6
- log_decay: float32 [512, 1024], P('sp', 'tp'), may hold values from -1 to 0
- span_state: float32 [8, 1024, 128], P('sp', 'tp'), may hold values from -6 to 6
Outputs:
- grad_w_gate: bfloat16 [4, 2048, 6144], P('sp', None, 'tp')
- grad_w_up: bfloat16 [4, 2048, 6144], P('sp', None, 'tp')
- grad_w_down: bfloat16 [4, 6144, 2048], P('sp', 'tp')
- grad_proj: float32 [2048, 2048], P('sp', 'tp')
- grad_queries: bfloat16 [512, 1024], P('sp', 'tp')
- grad_keys: bfloat16 [512, 1024], P('sp', 'tp')
- grad_values: bfloat16 [512, 2048], P('sp', 'tp')
- grad_decay: float32 [512, 1024], P('sp', 'tp')
Inputs may be any that keep to these rules, and one draw needn't show every extreme that they name: `route_expert`: each row names two different experts. Within the 128 rows of one index of sp no expert is named by more than 128 rows, a bound that some block reaches.
All inputs are finite; a program needn't handle non-finite values.
Results may differ from a plain program's by a relative error of at most 0.019.
Values may be sent and summed in bfloat16 or wider, within the bound.
A program may use at most 128 MiB of HBM per device.

v0:
```python
import jax
import jax.numpy as jnp
from jax import lax
from jax.sharding import PartitionSpec as P

DK = 64
SPAN = 64


HIGH = lax.Precision.HIGHEST


def entering(shard, axis, combine, identity):
    length, mine = (lax.axis_size(axis), lax.axis_index(axis))
    everything = jax.tree.map(lambda part: lax.all_gather(part, axis), shard)
    start = jax.tree.map(
        lambda part, zero: jnp.broadcast_to(jnp.asarray(zero, part.dtype), part.shape),
        shard,
        identity,
    )

    def step(k, before):
        at = length - 1 - k
        reached = at > mine
        new = combine(before, jax.tree.map(lambda part: part[at], everything))
        return jax.tree.map(lambda a, b: jnp.where(reached, a, b), new, before)

    return lax.fori_loop(0, length, step, start)


def slot_places(experts, count):
    routes_flat = experts.reshape(-1)
    one_hot = (routes_flat[:, None] == jnp.arange(count, dtype=jnp.int32)[None, :]).astype(
        jnp.int32
    )
    earlier = jnp.cumsum(one_hot, axis=0) - one_hot
    return jnp.sum(earlier * one_hot, axis=1).reshape(experts.shape)


def expert_grads(inputs, routed, gate_weight, up_weight, down_weight):
    gate = jnp.dot(inputs, gate_weight, preferred_element_type=jnp.float32)
    upper = jnp.dot(inputs, up_weight, preferred_element_type=jnp.float32)
    sigmoid_gate = jax.nn.sigmoid(gate)
    active = gate * sigmoid_gate
    hidden = (active * upper).astype(jnp.bfloat16)
    d_hidden = lax.dot_general(
        routed, down_weight, (((1,), (1,)), ((), ())), preferred_element_type=jnp.float32
    )
    d_upper = (d_hidden * active).astype(jnp.bfloat16)
    d_gate = (d_hidden * upper * sigmoid_gate * (1.0 + gate * (1.0 - sigmoid_gate))).astype(
        jnp.bfloat16
    )
    grad_down = lax.dot_general(
        hidden, routed, (((0,), (0,)), ((), ())), preferred_element_type=jnp.float32
    ).astype(jnp.bfloat16)
    grad_gate = lax.dot_general(
        inputs, d_gate, (((0,), (0,)), ((), ())), preferred_element_type=jnp.float32
    ).astype(jnp.bfloat16)
    grad_up = lax.dot_general(
        inputs, d_upper, (((0,), (0,)), ((), ())), preferred_element_type=jnp.float32
    ).astype(jnp.bfloat16)
    return (d_gate, d_upper, grad_gate, grad_up, grad_down)


def input_grad(d_gate, d_upper, gate_weight, up_weight):
    first = lax.dot_general(
        d_gate, gate_weight, (((1,), (1,)), ((), ())), preferred_element_type=jnp.float32
    )
    second = lax.dot_general(
        d_upper, up_weight, (((1,), (1,)), ((), ())), preferred_element_type=jnp.float32
    )
    return first + second


def gated_pieces(queries, keys, values, log_decay, grad_mix, key_dim, span_len):
    value_dim = values.shape[1] * key_dim // queries.shape[1]
    heads = queries.shape[1] // key_dim
    spans = queries.shape[0] // span_len

    def blocks(array, width):
        return array.astype(jnp.float32).reshape(spans, span_len, heads, width)

    query_spans = blocks(queries, key_dim)
    key_spans = blocks(keys, key_dim)
    value_spans = blocks(values, value_dim)
    grad_spans = blocks(grad_mix, value_dim)
    cumulative = jnp.cumsum(blocks(log_decay, key_dim), axis=1)
    last = cumulative[:, -1]
    scale = key_dim ** (-0.5)
    query_decayed = query_spans * jnp.exp(cumulative)
    key_grown = key_spans * jnp.exp(-cumulative)
    key_to_end = key_spans * jnp.exp(last[:, None] - cumulative)
    g_local = scale * jnp.einsum("nthk,nthv->nhkv", query_decayed, grad_spans, precision=HIGH)
    return (
        query_spans,
        key_spans,
        value_spans,
        grad_spans,
        cumulative,
        last,
        query_decayed,
        key_grown,
        key_to_end,
        g_local,
    )


def backward_step(carry, inputs):
    local, decay = inputs
    return (local + jnp.exp(decay)[..., None] * carry, carry)


def gated_finish(pieces, span_state, g_end, key_dim):
    (
        query_spans,
        key_spans,
        value_spans,
        grad_spans,
        cumulative,
        last,
        query_decayed,
        key_grown,
        key_to_end,
        g_local,
    ) = pieces
    spans, span_len, heads, value_dim = value_spans.shape
    scale = key_dim ** (-0.5)
    token_locations = jnp.arange(span_len, dtype=jnp.int32)
    causal = (token_locations[:, None] >= token_locations[None, :]).astype(jnp.float32)
    scores = jnp.einsum("nthk,nshk->nhts", query_decayed, key_grown, precision=HIGH) * causal
    grad_dot = jnp.einsum("nthv,nshv->nhts", grad_spans, value_spans, precision=HIGH) * causal
    state = span_state.reshape(spans, heads, key_dim, value_dim)
    d_query = (
        scale
        * jnp.exp(cumulative)
        * (
            jnp.einsum("nhts,nshk->nthk", grad_dot, key_grown, precision=HIGH)
            + jnp.einsum("nthv,nhkv->nthk", grad_spans, state, precision=HIGH)
        )
    )
    d_key = scale * jnp.exp(-cumulative) * jnp.einsum(
        "nhts,nthk->nshk", grad_dot, query_decayed, precision=HIGH
    ) + jnp.exp(last[:, None] - cumulative) * jnp.einsum(
        "nshv,nhkv->nshk", value_spans, g_end, precision=HIGH
    )
    d_value = scale * jnp.einsum(
        "nhts,nthv->nshv", scores, grad_spans, precision=HIGH
    ) + jnp.einsum("nshk,nhkv->nshv", key_to_end, g_end, precision=HIGH)
    state_end = jnp.exp(last)[..., None] * state + jnp.einsum(
        "nshk,nshv->nhkv", key_to_end, value_spans, precision=HIGH
    )
    tail = jnp.sum(state_end * g_end, axis=-1)
    d_cumulative = query_spans * d_query - key_spans * d_key
    d_log = jnp.cumsum(d_cumulative[:, ::-1], axis=1)[:, ::-1] + tail[:, None]
    rows = spans * span_len
    return (
        d_query.reshape(rows, heads * key_dim).astype(jnp.bfloat16),
        d_key.reshape(rows, heads * key_dim).astype(jnp.bfloat16),
        d_value.reshape(rows, heads * value_dim).astype(jnp.bfloat16),
        d_log.reshape(rows, heads * key_dim),
    )


def carry_combine(earlier, later):
    return (later[0] * earlier[0], later[1] + later[0][..., None] * earlier[1])


def on_device(
    moe_input,
    cotangent,
    route_expert,
    route_weight,
    w_gate,
    w_up,
    w_down,
    out_proj,
    saved_out,
    queries,
    keys,
    values,
    log_decay,
    span_state,
):
    tok_rows, width = moe_input.shape
    groups = lax.axis_size("sp")
    lanes = lax.axis_size("tp")
    capacity = 4 * tok_rows // groups
    target_locations = slot_places(route_expert, groups)
    rows_index = (target_locations * groups + route_expert).reshape(-1)
    owner = (
        jnp.full((capacity * groups,), 2 * tok_rows, jnp.int32)
        .at[rows_index]
        .set(jnp.arange(2 * tok_rows, dtype=jnp.int32))
    )
    weighted = (route_weight[:, :, None] * cotangent[:, None, :].astype(jnp.float32)).astype(
        jnp.bfloat16
    )
    weighted = weighted.reshape(2 * tok_rows, width)
    blank = jnp.zeros((1, width), jnp.bfloat16)
    send_in = jnp.concatenate([moe_input, blank], axis=0)[owner // 2].reshape(
        capacity, groups, width
    )
    send_cot = jnp.concatenate([weighted, blank], axis=0)[owner].reshape(capacity, groups, width)
    gate_weight = w_gate[0]
    up_weight = w_up[0]
    down_weight = w_down[0]
    share = capacity // lanes
    lane = lax.axis_index("tp")
    part_in = lax.dynamic_slice_in_dim(send_in, lane * share, share, 0)
    part_cot = lax.dynamic_slice_in_dim(send_cot, lane * share, share, 0)
    got_in, got_cot = (
        lax.all_to_all(part_in, "sp", split_axis=1, concat_axis=1, tiled=True),
        lax.all_to_all(part_cot, "sp", split_axis=1, concat_axis=1, tiled=True),
    )
    full_in, full_cot = (
        lax.all_gather(got_in, "tp", axis=0, tiled=True),
        lax.all_gather(got_cot, "tp", axis=0, tiled=True),
    )
    d_gate, d_upper, grad_gate, grad_up, grad_down = expert_grads(
        full_in.reshape(-1, width), full_cot.reshape(-1, width), gate_weight, up_weight, down_weight
    )
    mine = (
        lax.psum_scatter(
            input_grad(d_gate, d_upper, gate_weight, up_weight).astype(jnp.bfloat16),
            "tp",
            scatter_dimension=0,
            tiled=True,
        )
        .astype(jnp.float32)
        .reshape(share, groups, width)
    )
    returned = (
        lax.all_to_all(mine.astype(jnp.bfloat16), "sp", split_axis=1, concat_axis=1, tiled=True)
        .astype(mine.dtype)
        .reshape(-1, width)
    )
    local_index = rows_index - lane * share * groups
    inside = (local_index >= 0) & (local_index < share * groups)
    picked = jnp.where(inside[:, None], returned[jnp.clip(local_index, 0, share * groups - 1)], 0.0)
    routed = jnp.sum(picked.reshape(tok_rows, 2, width), axis=1)
    total = lax.psum(routed.astype(jnp.bfloat16), "tp").astype(jnp.float32)
    grad_in = (cotangent.astype(jnp.float32) + total).astype(jnp.bfloat16)
    grad_mix = lax.dot_general(
        grad_in, out_proj, (((1,), (1,)), ((), ())), preferred_element_type=jnp.float32
    )
    grad_proj = lax.psum_scatter(
        lax.dot_general(
            grad_in, saved_out, (((0,), (0,)), ((), ())), preferred_element_type=jnp.float32
        ).astype(jnp.bfloat16),
        "sp",
        scatter_dimension=0,
        tiled=True,
    ).astype(jnp.float32)
    pieces = gated_pieces(queries, keys, values, log_decay, grad_mix, DK, SPAN)
    g_local = pieces[9]
    last = pieces[5]
    begin = jnp.zeros(g_local.shape[1:], jnp.float32)
    device_start, local_end = lax.scan(backward_step, begin, (g_local, last), reverse=True)
    device_decay = jnp.exp(jnp.sum(last, axis=0))
    identity = (jnp.ones_like(device_decay), jnp.zeros_like(device_start))
    decay_after, state_after = entering((device_decay, device_start), "sp", carry_combine, identity)
    running = jnp.cumsum(last, axis=0)
    beyond = running[-1][None] - running
    g_end = local_end + jnp.exp(beyond)[..., None] * state_after[None]
    grad_queries, grad_keys, grad_values, grad_decay = gated_finish(pieces, span_state, g_end, DK)
    return (
        grad_gate[None],
        grad_up[None],
        grad_down[None],
        grad_proj,
        grad_queries,
        grad_keys,
        grad_values,
        grad_decay,
    )


def solution(mesh):
    placed = (
        P("sp", None),
        P("sp", None),
        P("sp", None),
        P("sp", None),
        P("sp", None, "tp"),
        P("sp", None, "tp"),
        P("sp", "tp", None),
        P("tp", None),
        P("sp", "tp"),
        P("sp", "tp"),
        P("sp", "tp"),
        P("sp", "tp"),
        P("sp", "tp"),
        P("sp", "tp", None),
    )
    return jax.shard_map(
        on_device,
        mesh=mesh,
        in_specs=placed,
        out_specs=(
            P("sp", None, "tp"),
            P("sp", None, "tp"),
            P("sp", "tp", None),
            P("sp", "tp"),
            P("sp", "tp"),
            P("sp", "tp"),
            P("sp", "tp"),
            P("sp", "tp"),
        ),
        check_vma=False,
    )
```

profile of v0, /device:TPU:0, one launch (start us, length us, event | category | flops | bytes accessed | tf_op | source)
XLA Modules:
  0.0 273.4 jit_solution(1842844893253880070)
XLA Ops:
  14.6 6.3 %gather_fusion = bf16[512,2048]{1,0:T(8,128)(2,1)} fusion(bf16[129,2048]{1,0:T(8,128)(2,1)} %concatenate.6, s32[1024]{0:T(1024)S(1)} %get-tuple-element.318), kind=kCustom, calls=%fused_computation | custom fusion | bytes 4196352 | tf_op jit(solution)/shard_map/gather | solution.py:200
  21.0 4.1 %reshape.208 = bf16[128,4,2048]{2,1,0:T(4,128)(2,1)} reshape(bf16[512,2048]{1,0:T(8,128)(2,1)} %gather_fusion) | data formatting | bytes 4194304 | tf_op jit(solution)/shard_map/reshape | solution.py:200
  26.3 10.7 %all_to_all.15 = bf16[16,4,2048]{2,0,1:T(8,128)(2,1)S(1)} all-to-all(bf16[16,4,2048]{2,0,1:T(8,128)(2,1)S(1)} %copy.146), channel_id=1, replica_groups=mesh['sp'=4,'tp'=8] {'sp'}, dimensions={1} | all-to-all | bytes 524288 | tf_op jit(solution)/shard_map/all_to_all | solution.py:212
  38.0 3.4 %mul.203 = f32[128,2,2048]{2,1,0:T(2,128)} broadcast(bf16[128,2048]{1,0:T(8,128)(2,1)} %param.19), dimensions={0,2} | broadcast | bytes 2621440 | tf_op jit(solution)/shard_map/mul | solution.py:195
  41.4 3.7 %mul.204 = f32[256,2048]{1,0:T(8,128)} reshape(f32[128,2,2048]{2,1,0:T(2,128)} %mul.203) | data formatting | bytes 4194304 | tf_op jit(solution)/shard_map/mul | solution.py:195
  48.3 6.6 %gather_fusion.1 = bf16[512,2048]{1,0:T(8,128)(2,1)} fusion(bf16[257,2048]{1,0:T(8,128)(2,1)} %concatenate.7, s32[1024]{0:T(1024)S(1)} %get-tuple-element.317), kind=kCustom, calls=%fused_computation.1 | custom fusion | bytes 4196352 | tf_op jit(solution)/shard_map/gather | solution.py:203
  54.9 4.1 %reshape.210 = bf16[128,4,2048]{2,1,0:T(4,128)(2,1)} reshape(bf16[512,2048]{1,0:T(8,128)(2,1)} %gather_fusion.1) | data formatting | bytes 4194304 | tf_op jit(solution)/shard_map/reshape | solution.py:203
  60.2 8.1 %all_to_all.16 = bf16[16,4,2048]{2,0,1:T(8,128)(2,1)S(1)} all-to-all(bf16[16,4,2048]{2,0,1:T(8,128)(2,1)S(1)} %copy.147), channel_id=1, replica_groups=mesh['sp'=4,'tp'=8] {'sp'}, dimensions={1} | all-to-all | bytes 524288 | tf_op jit(solution)/shard_map/all_to_all | solution.py:213
  69.5 3.9 %reshape.209 = bf16[512,2048]{1,0:T(8,128)(2,1)} reshape(bf16[128,4,2048]{2,1,0:T(4,128)(2,1)} %all-gather.6.cloned.1.call-done) | data formatting | bytes 4194304 | tf_op jit(solution)/shard_map/reshape | solution.py:220
  73.5 4.7 %fusion.3 = f32[512,768]{1,0:T(8,128)} fusion(bf16[512,2048]{1,0:T(8,128)(2,1)} %reshape.209, bf16[1,2048,768]{2,1,0:T(8,128)(2,1)S(1)} %copy-done), kind=kOutput, calls=%fused_computation.16 | convolution fusion | flops 1610612736 | bytes 6815744 | tf_op jit(solution)/shard_map/dot_general | solution.py:41
  81.1 17.2 %all-gather.8.cloned.1.call-done = bf16[128,4,2048]{2,1,0:T(4,128)(2,1)} async-done(((bf16[16,4,2048]{2,1,0:T(4,128)(2,1)}), bf16[128,4,2048]{2,1,0:T(4,128)(2,1)}) %all-gather.8.cloned.1.call-update) | async-done | bytes 2097168 | tf_op jit(solution)/shard_map/all_gather | solution.py:217
  98.3 3.9 %reshape.211 = bf16[512,2048]{1,0:T(8,128)(2,1)} reshape(bf16[128,4,2048]{2,1,0:T(4,128)(2,1)} %all-gather.8.cloned.1.call-done) | data formatting | bytes 4194304 | tf_op jit(solution)/shard_map/reshape | solution.py:220
  102.3 5.6 %multiply_convert_fusion.2 = (bf16[512,768]{1,0:T(8,128)(2,1)S(1)}, bf16[512,768]{1,0:T(8,128)(2,1)S(1)}) fusion(f32[512,768]{1,0:T(8,128)} %fusion.3, f32[512,768]{1,0:T(8,128)} %fusion.7, bf16[512,2048]{1,0:T(8,128)(2,1)} %reshape.211, bf16[1,768,2048]{2,1,0:T(8,128)(2,1)} %param.24), kind=kOutput, calls=%fused_computation.31 | convolution fusion | flops 1615724544 | bytes 9961472 | tf_op jit(solution)/shard_map/dot_general | solution.py:46
  110.4 3.2 %add_convert_fusion = bf16[512,2048]{1,0:T(8,128)(2,1)} fusion(f32[512,2048]{1,0:T(8,128)S(1)} %fusion.1, bf16[512,768]{1,0:T(8,128)(2,1)S(1)} %get-tuple-element.305, bf16[1,2048,768]{2,1,0:T(8,128)(2,1)S(1)} %copy-done.18), kind=kOutput, calls=%fused_computation.10 | convolution fusion | flops 1612709888 | bytes 10223616 | tf_op jit(solution)/shard_map/dot_general | solution.py:69
  115.3 8.0 %all-gather.2 = f32[4,2,64]{2,1,0:T(2,128)S(1)} all-gather(f32[1,2,64]{2,1,0:T(2,128)S(1)} %exponential_bitcast_fusion.1), channel_id=3, replica_groups=mesh['sp'=4,'tp'=8] {'sp'}, dimensions={0}, use_global_device_ids=true | all-gather | bytes 2560 | tf_op jit(solution)/shard_map/all_gather | solution.py:15
  124.4 6.3 %fusion.13 = bf16[1,768,2048]{2,1,0:T(8,128)(2,1)} fusion(bf16[512,2048]{1,0:T(8,128)(2,1)} %reshape.211, f32[512,768]{1,0:T(8,128)} %fusion.7, f32[512,768]{1,0:T(8,128)} %fusion.3), kind=kOutput, calls=%fused_computation.26 | convolution fusion | flops 1614544896 | bytes 8388608 | tf_op jit(solution)/shard_map/dot_general | solution.py:53
  130.7 18.3 %reduce-scatter.3.cloned.1.call-done = bf16[64,2048]{1,0:T(8,128)(2,1)} async-done(((bf16[512,2048]{1,0:T(8,128)(2,1)}), bf16[64,2048]{1,0:T(8,128)(2,1)}) %reduce-scatter.3.cloned.1.call-update) | async-done | bytes 262160 | tf_op jit(solution)/shard_map/reduce_scatter | solution.py:223
  150.9 3.8 %all-to-all-start.2 = ((bf16[16,4,2048]{2,0,1:T(8,128)(2,1)}), bf16[16,4,2048]{2,0,1:T(8,128)(2,1)S(1)}, u32[]{:S(2)}, u32[]{:S(2)}) async-start(bf16[16,4,2048]{2,0,1:T(8,128)(2,1)} %copy.115), calls=%async_computation.3 | async-start | bytes 524288 | tf_op jit(solution)/shard_map/all_to_all | solution.py:233
  154.7 4.6 %fusion.12 = bf16[1,2048,768]{2,1,0:T(8,128)(2,1)} fusion(bf16[512,2048]{1,0:T(8,128)(2,1)S(1)} %copy-done.5, bf16[512,768]{1,0:T(8,128)(2,1)} %copy-done.19), kind=kOutput, calls=%fused_computation.25 | convolution fusion | flops 1612185600 | bytes 6029312 | tf_op jit(solution)/shard_map/dot_general | solution.py:59
  164.2 5.8 %select_reduce_fusion = bf16[128,2048]{1,0:T(8,128)(2,1)} fusion(f32[128,2,2048]{2,1,0:T(2,128)} %gather.14, pred[128,2]{1,0:T(8,128)(4,1)S(1)} %copy.114), kind=kLoop, calls=%fused_computation.28 | loop fusion | flops 786432 | bytes 2621696 | tf_op jit(solution)/shard_map/reduce_sum | solution.py:240
  170.2 4.7 %fusion.11 = bf16[1,2048,768]{2,1,0:T(8,128)(2,1)} fusion(bf16[512,2048]{1,0:T(8,128)(2,1)S(1)} %copy-done.6, bf16[512,768]{1,0:T(8,128)(2,1)} %copy-done.20), kind=kOutput, calls=%fused_computation.24 | convolution fusion | flops 1612185600 | bytes 6029312 | tf_op jit(solution)/shard_map/dot_general | solution.py:56
  174.9 49.9 %all-reduce.4.cloned.1.call-done = bf16[128,2048]{1,0:T(8,128)(2,1)} async-done(((bf16[128,2048]{1,0:T(8,128)(2,1)}), bf16[128,2048]{1,0:T(8,128)(2,1)}) %all-reduce.4.cloned.1.call-update) | async-done | bytes 524304 | tf_op jit(solution)/shard_map/psum | solution.py:241
  227.4 9.5 %all-gather = f32[8,64,128]{2,1,0:T(8,128)S(1)} all-gather(f32[2,64,128]{2,1,0:T(8,128)S(1)} %get-tuple-element.245), channel_id=2, replica_groups=mesh['sp'=4,'tp'=8] {'sp'}, dimensions={0}, use_global_device_ids=true | all-gather | bytes 327680 | tf_op jit(solution)/shard_map/all_gather | solution.py:15
  255.4 9.7 %reduce-scatter.5.cloned.1.call-done = bf16[512,256]{1,0:T(8,128)(2,1)} async-done(((bf16[2048,256]{1,0:T(8,128)(2,1)}), bf16[512,256]{1,0:T(8,128)(2,1)}) %reduce-scatter.5.cloned.1.call-update) | async-done | bytes 262160 | tf_op jit(solution)/shard_map/reduce_scatter | solution.py:246
  (157 shorter events, 53.4 us)
Async XLA Ops:
  7.2 66.3 %copy-start = (bf16[1,2048,768]{2,1,0:T(8,128)(2,1)S(1)}, bf16[1,2048,768]{2,1,0:T(8,128)(2,1)}, u32[]{:S(2)}) copy-start(bf16[1,2048,768]{2,1,0:T(8,128)(2,1)} %param.22) | copy-start | bytes 9437188
  7.2 62.3 %all-gather.6.cloned.1.call-start = ((), (), s32[]{:S(2)}) async-start(), calls=%async_computation.5 | async-start | bytes 2359296 | tf_op jit(solution)/shard_map/all_gather | solution.py:216
  38.0 60.4 %all-gather.8.cloned.1.call-start = ((), (), s32[]{:S(2)}) async-start(), calls=%async_computation.6 | async-start | bytes 2359296 | tf_op jit(solution)/shard_map/all_gather | solution.py:217
  41.4 3.7 %copy-start.16 = (f32[128,2]{0,1:T(2,128)S(1)}, f32[128,2]{0,1:T(2,128)}, u32[]{:S(2)}) copy-start(f32[128,2]{0,1:T(2,128)} %param.21) | copy-start | bytes 3076
  69.3 79.7 %reduce-scatter.3.cloned.1.call-start = ((), (), s32[]{:S(2)}) async-start(), calls=%async_computation.7 | async-start | bytes 2359296 | tf_op jit(solution)/shard_map/reduce_scatter | solution.py:223
  73.5 4.7 %copy-start.4 = (bf16[512,2048]{1,0:T(8,128)(2,1)S(1)}, bf16[512,2048]{1,0:T(8,128)(2,1)}, u32[]{:S(2)}) copy-start(bf16[512,2048]{1,0:T(8,128)(2,1)} %reshape.209) | copy-start | bytes 6291460
  73.5 4.7 %copy-start.17 = (bf16[1,2048,768]{2,1,0:T(8,128)(2,1)S(1)}, bf16[1,2048,768]{2,1,0:T(8,128)(2,1)}, u32[]{:S(2)}) copy-start(bf16[1,2048,768]{2,1,0:T(8,128)(2,1)} %param.23) | copy-start | bytes 9437188
  107.9 1.9 copy-start.20
  107.9 1.9 copy-start.19
  107.9 2.5 copy-start.18
  113.6 1.7 copy-start.13
  124.4 30.3 %copy-start.5 = (bf16[512,2048]{1,0:T(8,128)(2,1)S(1)}, bf16[512,2048]{1,0:T(8,128)(2,1)}, u32[]{:S(2)}) copy-start(bf16[512,2048]{1,0:T(8,128)(2,1)} %reshape.209) | copy-start | bytes 6291460
  150.9 9.2 %all-to-all-start.2 = ((bf16[16,4,2048]{2,0,1:T(8,128)(2,1)}), bf16[16,4,2048]{2,0,1:T(8,128)(2,1)S(1)}, u32[]{:S(2)}, u32[]{:S(2)}) async-start(bf16[16,4,2048]{2,0,1:T(8,128)(2,1)} %copy.115), calls=%async_computation.3 | async-start | bytes 524288 | tf_op jit(solution)/shard_map/all_to_all | solution.py:233
  154.7 70.0 %all-reduce.4.cloned.1.call-start = ((), (), s32[]{:S(2)}) async-start(), calls=%async_computation.8 | async-start | bytes 1048576 | tf_op jit(solution)/shard_map/psum | solution.py:241
  164.2 5.9 %copy-start.6 = (bf16[512,2048]{1,0:T(8,128)(2,1)S(1)}, bf16[512,2048]{1,0:T(8,128)(2,1)}, u32[]{:S(2)}) copy-start(bf16[512,2048]{1,0:T(8,128)(2,1)} %reshape.209) | copy-start | bytes 6291460
  170.1 54.6 %copy-start.2 = (bf16[128,2048]{1,0:T(8,128)(2,1)S(1)}, bf16[128,2048]{1,0:T(8,128)(2,1)}, u32[]{:S(2)}) copy-start(bf16[128,2048]{1,0:T(8,128)(2,1)} %param.19) | copy-start | bytes 1572868
  170.1 95.0 %reduce-scatter.5.cloned.1.call-start = ((), (), s32[]{:S(2)}) async-start(), calls=%async_computation.9 | async-start | bytes 1310720 | tf_op jit(solution)/shard_map/reduce_scatter | solution.py:246
  226.6 10.8 %copy-start.7 = (bf16[128,2048]{1,0:T(8,128)(2,1)S(1)}, bf16[128,2048]{1,0:T(8,128)(2,1)}, u32[]{:S(2)}) copy-start(bf16[128,2048]{1,0:T(8,128)(2,1)} %all-reduce.4.cloned.1.call-done) | copy-start | bytes 1572868
  226.6 10.8 %copy-start.12 = (bf16[128,256]{1,0:T(8,128)(2,1)S(1)}, bf16[128,256]{1,0:T(8,128)(2,1)}, u32[]{:S(2)}) copy-start(bf16[128,256]{1,0:T(8,128)(2,1)} %param.26) | copy-start | bytes 196612
  226.7 12.5 %copy-start.3 = (f32[2,64,2,128]{3,2,1,0:T(2,128)}, f32[2,64,2,128]{3,2,1,0:T(2,128)S(1)}, u32[]{:S(2)}) copy-start(f32[2,64,2,128]{3,2,1,0:T(2,128)S(1)} %reshape.217) | copy-start | bytes 393220
  227.4 12.2 %copy-start.8 = (f32[2,2,64,128]{3,2,1,0:T(8,128)}, f32[2,2,64,128]{3,2,1,0:T(8,128)S(1)}, u32[]{:S(2)}) copy-start(f32[2,2,64,128]{3,2,1,0:T(8,128)S(1)} %get-tuple-element.244) | copy-start | bytes 393220
  237.5 1.7 copy-start.9
  241.2 25.7 %copy-start.1 = (bf16[1,2048,768]{2,1,0:T(8,128)(2,1)S(1)}, bf16[1,2048,768]{2,1,0:T(8,128)(2,1)}, u32[]{:S(2)}) copy-start(bf16[1,2048,768]{2,1,0:T(8,128)(2,1)} %param.22) | copy-start | bytes 9437188
  246.1 8.5 %copy-start.10 = (bf16[2,64,2,64]{1,3,2,0:T(8,128)(2,1)S(1)}, bf16[2,64,2,64]{1,3,2,0:T(8,128)(2,1)}, u32[]{:S(2)}) copy-start(bf16[2,64,2,64]{1,3,2,0:T(8,128)(2,1)} %get-tuple-element.309) | copy-start | bytes 98308
  (3 other events, 3.4 us)
Sparse Core Ops, SparseCore 0:
  38.1 28.8 all-gather.5
  69.4 28.8 all-gather.7
  113.7 35.2 reduce-scatter.2
  170.2 54.4 all-reduce.3
  239.1 26.0 reduce-scatter.4
where the time goes:
time: 275 us; the launch traced here: 273 us
  waiting for transfers between devices  95.9 us (35%)
  local copies, waits for them, and re-layouts  63.6 us (23%)
  matrix products  44.8 us (16%)
  blocking collectives  36.4 us (13%)
  between operations  14.4 us (5%)
  other arithmetic  14 us (5%)
  starting transfers between devices  4.16 us (2%)
    psum x1, waiting for transfers between devices, on_device(): total = lax.psum(routed.astype(jnp.bfloat16), 'tp').astype(jnp.float32)  49.9 us
    reduce_scatter x1, waiting for transfers between devices, on_device(): lax.psum_scatter(input_grad(d_gate, d_upper, gate_weight, up_weight).asty...  18.3 us
    all_gather x2, blocking collectives, entering(): everything = jax.tree.map(lambda part: lax.all_gather(part, axis), shard)  17.5 us
    all_gather x1, waiting for transfers between devices, on_device(): lax.all_gather(got_cot, 'tp', axis=0, tiled=True)  17.2 us
    all_to_all x1, blocking collectives, on_device(): lax.all_to_all(part_in, 'sp', split_axis=1, concat_axis=1, tiled=True)  10.7 us
    reduce_scatter x1, waiting for transfers between devices, on_device(): lax.psum_scatter(lax.dot_general(grad_in, saved_out, (((0,), (0,)), ((),...  9.71 us
    all_to_all x1, blocking collectives, on_device(): lax.all_to_all(part_cot, 'sp', split_axis=1, concat_axis=1, tiled=True)  8.11 us
    mul x3, local copies, waits for them, and re-layouts, on_device(): route_weight[:, :, None] * cotangent[:, None, :].astype(jnp.float32)  7.21 us
  transfers between devices with their start and end apart: 6, of which 5 were waited for; matrix products, arithmetic and copies ran while one was open for 25% of the time, Pallas kernels for 0%

commit v1 on v0

v1 whole, which is shorter than its diff:
```python
import functools

import jax
import jax.numpy as jnp
from jax import lax
from jax.experimental import pallas as pl
from jax.experimental.pallas import tpu as pltpu
from jax.sharding import PartitionSpec as P

DK = 64
SPAN = 64

HIGH = lax.Precision.HIGHEST
F32 = jnp.float32
BF16 = jnp.bfloat16


def dot(a, b, dims, precision=HIGH):
    return lax.dot_general(
        a, b, ((dims[0], dims[1]), ((), ())), precision=precision, preferred_element_type=F32
    )


NN = ((1,), (0,))
NT = ((1,), (1,))
TN = ((0,), (0,))


def triangle(size, upper):
    row = lax.broadcasted_iota(jnp.int32, (size, size), 0)
    col = lax.broadcasted_iota(jnp.int32, (size, size), 1)
    return ((row <= col) if upper else (row >= col)).astype(F32)


def mix_kernel(grad_in, out_proj, queries, log_decay, mix_out, start_out):
    mix = dot(grad_in[...], out_proj[...], NT, None)
    mix_out[...] = mix
    rows, channels = queries.shape
    heads = channels // DK
    wide = mix.shape[1] // heads
    lower = triangle(SPAN, False)
    ones = jnp.ones((SPAN, wide), F32)
    for h in range(heads):
        keyed = slice(h * DK, (h + 1) * DK)
        carry = None
        for n in reversed(range(rows // SPAN)):
            at = slice(n * SPAN, (n + 1) * SPAN)
            decay = log_decay[at, keyed]
            qd = queries[at, keyed].astype(F32) * jnp.exp(dot(lower, decay, NN))
            local = DK**-0.5 * dot(qd, mix[at, h * wide : (h + 1) * wide], TN)
            if carry is not None:
                local = local + jnp.exp(dot(decay, ones, TN)) * carry
            carry = local
        start_out[keyed, :] = carry


def finish_kernel(queries, keys, values, log_decay, mix, state, after, dq_o, dk_o, dv_o, dl_o):
    rows, channels = queries.shape
    heads = channels // DK
    wide = values.shape[1] // heads
    lower = triangle(SPAN, False)
    upper = triangle(SPAN, True)
    ones = jnp.ones((SPAN, wide), F32)
    scale = DK**-0.5
    for h in range(heads):
        keyed = slice(h * DK, (h + 1) * DK)
        valued = slice(h * wide, (h + 1) * wide)
        g_end = after[keyed, :]
        for n in reversed(range(rows // SPAN)):
            at = slice(n * SPAN, (n + 1) * SPAN)
            q = queries[at, keyed].astype(F32)
            k = keys[at, keyed].astype(F32)
            v = values[at, valued].astype(F32)
            g = mix[at, valued]
            s0 = state[n, keyed, :]
            decay = log_decay[at, keyed]
            c = dot(lower, decay, NN)
            last = c[SPAN - 1 : SPAN, :]
            grow, shrink, to_end = jnp.exp(c), jnp.exp(-c), jnp.exp(last - c)
            qd, kd, ke = q * grow, k * shrink, k * to_end
            scores = dot(qd, kd, NT) * lower
            gv = dot(g, v, NT) * lower
            dq = scale * grow * (dot(gv, kd, NN) + dot(g, s0, NT))
            dk = scale * shrink * dot(gv, qd, TN) + to_end * dot(v, g_end, NT)
            dv = scale * dot(scores, g, TN) + dot(ke, g_end, NN)
            e_last = jnp.exp(dot(decay, ones, TN))
            s1 = e_last * s0 + dot(ke, v, TN)
            dq_o[at, keyed] = dq.astype(BF16)
            dk_o[at, keyed] = dk.astype(BF16)
            dv_o[at, valued] = dv.astype(BF16)
            dl_o[at, keyed] = dot(upper, q * dq - k * dk, NN) + dot(ones, s1 * g_end, NT)
            if n:
                g_end = DK**-0.5 * dot(qd, g, TN) + e_last * g_end


def call(kernel, outs, *args):
    return pl.pallas_call(
        kernel,
        out_shape=[jax.ShapeDtypeStruct(s, d) for s, d in outs],
        in_specs=[pl.BlockSpec(memory_space=pltpu.VMEM)] * len(args),
        out_specs=[pl.BlockSpec(memory_space=pltpu.VMEM)] * len(outs),
        cost_estimate=pl.CostEstimate(flops=2 * 10**8, bytes_accessed=10**6, transcendentals=0),
    )(*args)


def on_device(
    moe_input,
    cotangent,
    route_expert,
    route_weight,
    w_gate,
    w_up,
    w_down,
    out_proj,
    saved_out,
    queries,
    keys,
    values,
    log_decay,
    span_state,
):
    tok_rows, width = moe_input.shape
    groups = lax.axis_size("sp")
    lanes = lax.axis_size("tp")
    me = lax.axis_index("sp")
    lane = lax.axis_index("tp")
    inputs = lax.all_gather(moe_input, "sp", axis=0, tiled=True)
    cots = lax.all_gather(cotangent, "sp", axis=0, tiled=True)
    named = route_expert[:, :, None] == jnp.arange(groups, dtype=jnp.int32)
    weights = jnp.sum(jnp.where(named, route_weight[:, :, None], 0.0), axis=1).T
    small = lax.all_gather(
        jnp.concatenate([weights.reshape(-1), jnp.sum(log_decay, axis=0)]), "sp"
    )
    weights_all = small[:, : groups * tok_rows].reshape(groups, groups, tok_rows)
    mine = lax.dynamic_index_in_dim(weights_all, me, 1, keepdims=False).reshape(-1, 1)
    decays = small[:, groups * tok_rows :]

    gate_weight, up_weight, down_weight = w_gate[0], w_up[0], w_down[0]
    gate = jnp.dot(inputs, gate_weight, preferred_element_type=F32)
    upper = jnp.dot(inputs, up_weight, preferred_element_type=F32)
    routed = (mine * cots.astype(F32)).astype(BF16)
    sigmoid_gate = jax.nn.sigmoid(gate)
    active = gate * sigmoid_gate
    hidden = (active * upper).astype(BF16)
    d_hidden = dot(routed, down_weight, NT, None)
    d_upper = (d_hidden * active).astype(BF16)
    d_gate = (d_hidden * upper * sigmoid_gate * (1.0 + gate * (1.0 - sigmoid_gate))).astype(BF16)
    slots = (dot(d_gate, gate_weight, NT, None) + dot(d_upper, up_weight, NT, None)).astype(BF16)
    part = lax.psum_scatter(slots, ("sp", "tp"), scatter_dimension=0, tiled=True)
    grad_down = dot(hidden, routed, TN, None).astype(BF16)
    grad_gate = dot(inputs, d_gate, TN, None).astype(BF16)
    grad_up = dot(inputs, d_upper, TN, None).astype(BF16)

    share = tok_rows // lanes
    own = lax.dynamic_slice_in_dim(cotangent, lane * share, share, 0)
    part = (own.astype(F32) + part.astype(F32)).astype(BF16)
    grad_in = lax.all_gather(part, "tp", axis=0, tiled=True)

    channels, wide = queries.shape[1], span_state.shape[2]
    mix, start = call(
        mix_kernel,
        [((tok_rows, values.shape[1]), F32), ((channels, wide), F32)],
        grad_in,
        out_proj,
        queries,
        log_decay,
    )
    starts = lax.all_gather(start, "sp")
    grad_proj = lax.psum_scatter(
        dot(grad_in, saved_out, TN, None).astype(BF16), "sp", scatter_dimension=0, tiled=True
    ).astype(F32)
    at = jnp.arange(groups, dtype=jnp.int32)
    between = ((at[None, :] > me) & (at[None, :] < at[:, None])).astype(F32)
    factor = jnp.exp(jnp.sum(between[:, :, None] * decays[None], axis=1))
    factor = jnp.where((at > me)[:, None], factor, 0.0)
    after = jnp.sum(factor[:, :, None] * starts, axis=0)
    grad_queries, grad_keys, grad_values, grad_decay = call(
        finish_kernel,
        [
            (queries.shape, BF16),
            (keys.shape, BF16),
            (values.shape, BF16),
            (log_decay.shape, F32),
        ],
        queries,
        keys,
        values,
        log_decay,
        mix,
        span_state,
        after,
    )
    return (
        grad_gate[None],
        grad_up[None],
        grad_down[None],
        grad_proj,
        grad_queries,
        grad_keys,
        grad_values,
        grad_decay,
    )


def solution(mesh):
    placed = (
        P("sp", None),
        P("sp", None),
        P("sp", None),
        P("sp", None),
        P("sp", None, "tp"),
        P("sp", None, "tp"),
        P("sp", "tp", None),
        P("tp", None),
        P("sp", "tp"),
        P("sp", "tp"),
        P("sp", "tp"),
        P("sp", "tp"),
        P("sp", "tp"),
        P("sp", "tp", None),
    )
    return jax.shard_map(
        on_device,
        mesh=mesh,
        in_specs=placed,
        out_specs=(
            P("sp", None, "tp"),
            P("sp", None, "tp"),
            P("sp", "tp", None),
            P("sp", "tp"),
            P("sp", "tp"),
            P("sp", "tp"),
            P("sp", "tp"),
            P("sp", "tp"),
        ),
        check_vma=False,
    )
```

time: 275 us -> 307 us (1.12)
  waiting for transfers between devices: 95.9 us -> 197 us
  local copies, waits for them, and re-layouts: 63.6 us -> 10.9 us
  Pallas kernels: 0 us -> 9.56 us
  other arithmetic: 14 us -> 5.19 us
  matrix products: 44.8 us -> 36.7 us
  starting transfers between devices: 4.16 us -> 0.16 us
  blocking collectives: 36.4 us -> 33.2 us
    reduce_scatter x2, waiting for transfers between devices: 28 us -> 139 us  [the longest x1 139 us: on_device(): lax.psum_scatter(slots, ('sp', 'tp'), scatter_dimension=0, tiled=True)]
    psum x1 -> x0, waiting for transfers between devices: 49.9 us -> none  [on_device(): total = lax.psum(routed.astype(jnp.bfloat16), 'tp').astype(jnp.float32)]
    all_gather x2, waiting for transfers between devices: 17.2 us -> 57.1 us  [the longest x1 29.3 us: on_device(): cots = lax.all_gather(cotangent, 'sp', axis=0, tiled=True)]
    reshape x15 -> x1, local copies, waits for them, and re-layouts: 18.9 us -> 0.02 us  [on_device(): weights_all = small[:, :groups * tok_rows].reshape(groups, groups, tok_rows)]
    all_to_all x2 -> x0, blocking collectives: 18.8 us -> none  [the longest x1 10.7 us: on_device(): lax.all_to_all(part_in, 'sp', split_axis=1, concat_axis=1, tiled=True)]
    gather x4 -> x0, local copies, waits for them, and re-layouts: 16.7 us -> none  [the longest x1 6.6 us: on_device(): jnp.concatenate([weighted, blank], axis=0)[owner]]
    all_gather x2 -> x3, blocking collectives: 17.5 us -> 33.2 us  [the longest x1 15.1 us: on_device(): grad_in = lax.all_gather(part, 'tp', axis=0, tiled=True)]
    pallas_call x0 -> x2, Pallas kernels: none -> 9.56 us  [call(): pl.pallas_call(kernel, out_shape=[jax.ShapeDtypeStruct(s, d) for s, d in...]
  transfers between devices with their start and end apart: 6 -> 4, of which waited for: 5 -> 3; matrix products, arithmetic and copies ran while one was open for 25% -> 12% of each run, Pallas kernels for 0% -> 3%
where the time goes in v1:
time: 307 us
  waiting for transfers between devices  197 us (64%)
  matrix products  36.7 us (12%)
  blocking collectives  33.2 us (11%)
  between operations  13.9 us (5%)
  local copies, waits for them, and re-layouts  10.9 us (4%)
  Pallas kernels  9.56 us (3%)
  other arithmetic  5.19 us (2%)
    reduce_scatter x1, waiting for transfers between devices, on_device(): lax.psum_scatter(slots, ('sp', 'tp'), scatter_dimension=0, tiled=True)  139 us
    all_gather x1, waiting for transfers between devices, on_device(): cots = lax.all_gather(cotangent, 'sp', axis=0, tiled=True)  29.3 us
    dot_general x7, matrix products, dot(): lax.dot_general(a, b, ((dims[0], dims[1]), ((), ())), precision=precision...  29 us
    all_gather x1, waiting for transfers between devices, on_device(): inputs = lax.all_gather(moe_input, 'sp', axis=0, tiled=True)  27.8 us
    all_gather x1, blocking collectives, on_device(): grad_in = lax.all_gather(part, 'tp', axis=0, tiled=True)  15.1 us
    unnamed x20, local copies, waits for them, and re-layouts  10.8 us
    all_gather x1, blocking collectives, on_device(): lax.all_gather(jnp.concatenate([weights.reshape(-1), jnp.sum(log_decay, a...  9.66 us
    pallas_call x2, Pallas kernels, call(): pl.pallas_call(kernel, out_shape=[jax.ShapeDtypeStruct(s, d) for s, d in...  9.56 us
  transfers between devices with their start and end apart: 4, of which 3 were waited for; matrix products, arithmetic and copies ran while one was open for 12% of the time, Pallas kernels for 3%

profile of v1, /device:TPU:0, one launch (start us, length us, event | category | flops | bytes accessed | tf_op | source)
XLA Modules:
  0.0 306.7 jit_solution(10002399446135464405)
XLA Ops:
  8.7 0.9 reduce_sum.37
  10.3 9.7 %all-gather.2 = f32[4,1,640]{2,1,0:T(1,128)S(1)} all-gather(f32[1,1,640]{2,1,0:T(1,128)S(1)} %reshape.85), channel_id=2, replica_groups=mesh['sp'=4,'tp'=8] {'sp'}, dimensions={0}, use_global_device_ids=true | all-gather | bytes 12800 | tf_op jit(solution)/shard_map/all_gather | solution.py:131
  20.0 27.8 %all-gather.8.cloned.1.call-done = bf16[512,2048]{1,0:T(8,128)(2,1)} async-done(((bf16[128,2048]{1,0:T(8,128)(2,1)}), bf16[512,2048]{1,0:T(8,128)(2,1)}) %all-gather.8.cloned.1.call-update) | async-done | bytes 2097168 | tf_op jit(solution)/shard_map/all_gather | solution.py:127
  47.8 4.7 %fusion.2 = f32[512,768]{1,0:T(8,128)} fusion(bf16[512,2048]{1,0:T(8,128)(2,1)} %all-gather.8.cloned.1.call-done, bf16[1,2048,768]{2,1,0:T(8,128)(2,1)S(1)} %copy-done), kind=kOutput, calls=%fused_computation.7 | convolution fusion | flops 1610612736 | bytes 6815744 | tf_op jit(solution)/shard_map/dot_general | solution.py:139
  52.5 3.0 fusion.6
  55.5 29.3 %all-gather.6.cloned.1.call-done = bf16[512,2048]{1,0:T(8,128)(2,1)} async-done(((bf16[128,2048]{1,0:T(8,128)(2,1)}), bf16[512,2048]{1,0:T(8,128)(2,1)}) %all-gather.6.cloned.1.call-update) | async-done | bytes 2097168 | tf_op jit(solution)/shard_map/all_gather | solution.py:128
  84.8 5.6 %multiply_convert_fusion.2 = (bf16[512,768]{1,0:T(8,128)(2,1)S(1)}, bf16[512,768]{1,0:T(8,128)(2,1)S(1)}) fusion(f32[512,768]{1,0:T(8,128)} %fusion.2, f32[512,768]{1,0:T(8,128)} %fusion.6, bf16[1,768,2048]{2,1,0:T(8,128)(2,1)} %param.20, bf16[512,2048]{1,0:T(8,128)(2,1)} %all-gather.6.cloned.1.call-done, f32[512]{0:T(512)S(1)} %bitcast.49), kind=kOutput, calls=%fused_computation.20 | convolution fusion | flops 1618870272 | bytes 9963520 | tf_op jit(solution)/shard_map/dot_general | solution.py:19
  90.5 1.8 fusion
  92.9 3.1 %add_convert_fusion = bf16[512,2048]{1,0:T(8,128)(2,1)} fusion(f32[512,2048]{1,0:T(8,128)S(1)} %fusion, bf16[512,768]{1,0:T(8,128)(2,1)S(1)} %get-tuple-element.52, bf16[1,2048,768]{2,1,0:T(8,128)(2,1)S(1)} %copy-done.4), kind=kOutput, calls=%fused_computation | convolution fusion | flops 1612709888 | bytes 10223616 | tf_op jit(solution)/shard_map/dot_general | solution.py:19
  96.2 138.6 %reduce-scatter.3.cloned.1.call-done = bf16[16,2048]{1,0:T(8,128)(2,1)} async-done(((bf16[512,2048]{1,0:T(8,128)(2,1)}), bf16[16,2048]{1,0:T(8,128)(2,1)}) %reduce-scatter.3.cloned.1.call-update) | async-done | bytes 65552 | tf_op jit(solution)/shard_map/reduce_scatter | solution.py:149
  234.8 0.9 add_convert_fusion.1
  235.7 15.1 %all_gather.25.grad_in = bf16[128,2048]{1,0:T(8,128)(2,1)S(1)} all-gather(bf16[16,2048]{1,0:T(8,128)(2,1)S(1)} %add_convert_fusion.1), channel_id=1, replica_groups=mesh['sp'=4,'tp'=8] {'tp'}, dimensions={0}, use_global_device_ids=true | all-gather | bytes 589824 | tf_op jit(solution)/shard_map/all_gather | solution.py:157
  250.9 0.8 copy-done.1
  251.6 1.5 convolution_convert_fusion.3
  253.3 5.3 %fusion.11 = bf16[1,2048,768]{1,2,0:T(8,128)(2,1)} fusion(bf16[512,768]{1,0:T(8,128)(2,1)} %copy-done.6, bf16[512,2048]{1,0:T(8,128)(2,1)} %all-gather.8.cloned.1.call-done), kind=kOutput, calls=%fused_computation.16 | convolution fusion | flops 1612185600 | bytes 6029312 | tf_op jit(solution)/shard_map/dot_general | solution.py:19
  258.7 4.6 %copy.35 = bf16[1,2048,768]{2,1,0:T(8,128)(2,1)} copy(bf16[1,2048,768]{1,2,0:T(8,128)(2,1)} %fusion.11) | data formatting | bytes 6291456
  263.3 5.3 %fusion.10 = bf16[1,2048,768]{1,2,0:T(8,128)(2,1)} fusion(bf16[512,768]{1,0:T(8,128)(2,1)} %copy-done.7, bf16[512,2048]{1,0:T(8,128)(2,1)} %all-gather.8.cloned.1.call-done), kind=kOutput, calls=%fused_computation.15 | convolution fusion | flops 1612185600 | bytes 6029312 | tf_op jit(solution)/shard_map/dot_general | solution.py:19
  268.7 4.7 %copy.34 = bf16[1,2048,768]{2,1,0:T(8,128)(2,1)} copy(bf16[1,2048,768]{1,2,0:T(8,128)(2,1)} %fusion.10) | data formatting | bytes 6291456
  273.4 6.2 %fusion.12 = bf16[1,768,2048]{2,1,0:T(8,128)(2,1)} fusion(bf16[512,2048]{1,0:T(8,128)(2,1)} %all-gather.6.cloned.1.call-done, f32[512]{0:T(512)S(1)} %bitcast.50, f32[512,768]{1,0:T(8,128)} %fusion.6, f32[512,768]{1,0:T(8,128)} %fusion.2), kind=kOutput, calls=%fused_computation.17 | convolution fusion | flops 1617690624 | bytes 8390656 | tf_op jit(solution)/shard_map/dot_general | solution.py:19
  279.6 4.1 %shard_map.197 = (f32[128,256]{1,0:T(8,128)}, f32[128,128]{1,0:T(8,128)}) custom-call(bf16[128,2048]{1,0:T(8,128)(2,1)} %copy-done.1, bf16[256,2048]{1,0:T(8,128)(2,1)} %out_proj.1, bf16[128,128]{1,0:T(8,128)(2,1)} %queries.3, f32[128,128]{1,0:T(8,128)} %log_decay.3), custom_call_target="tpu_custom_call" | custom-call | flops 200000000 | bytes 1000000 | tf_op jit(solution)/shard_map/pallas_call | solution.py:97
  283.8 8.4 %all-gather.1 = f32[512,128]{1,0:T(8,128)S(1)} all-gather(f32[128,128]{1,0:T(8,128)} %get-tuple-element.15), channel_id=3, replica_groups=mesh['sp'=4,'tp'=8] {'sp'}, dimensions={0}, use_global_device_ids=true | all-gather | bytes 327680 | tf_op jit(solution)/shard_map/all_gather | solution.py:168
  292.2 0.8 multiply_reduce_fusion.after
  292.9 5.4 %shard_map.198 = (bf16[128,128]{1,0:T(8,128)(2,1)}, bf16[128,128]{1,0:T(8,128)(2,1)}, bf16[128,256]{1,0:T(8,128)(2,1)}, f32[128,128]{1,0:T(8,128)}) custom-call(bf16[128,128]{1,0:T(8,128)(2,1)} %queries.3, bf16[128,128]{1,0:T(8,128)(2,1)} %keys.1, bf16[128,256]{1,0:T(8,128)(2,1)} %values.1, f32[128,128]{1,0:T(8,128)} %log_decay.3, ...), custom_call_target="tpu_custom_call" | custom-call | flops 200000000 | bytes 1000000 | tf_op jit(solution)/shard_map/pallas_call | solution.py:97
  298.4 1.8 convert_element_type.70
  (36 shorter events, 3.1 us)
Async XLA Ops:
  7.2 40.6 %copy-start = (bf16[1,2048,768]{2,1,0:T(8,128)(2,1)S(1)}, bf16[1,2048,768]{2,1,0:T(8,128)(2,1)}, u32[]{:S(2)}) copy-start(bf16[1,2048,768]{2,1,0:T(8,128)(2,1)} %param.18) | copy-start | bytes 9437188
  7.2 40.6 %all-gather.8.cloned.1.call-start = ((), (), s32[]{:S(2)}) async-start(), calls=%async_computation.3 | async-start | bytes 2621440 | tf_op jit(solution)/shard_map/all_gather | solution.py:127
  7.9 76.9 %all-gather.6.cloned.1.call-start = ((), (), s32[]{:S(2)}) async-start(), calls=%async_computation.2 | async-start | bytes 2621440 | tf_op jit(solution)/shard_map/all_gather | solution.py:128
  8.7 226.2 %reduce-scatter.3.cloned.1.call-start = ((), (), s32[]{:S(2)}) async-start(), calls=%async_computation.4 | async-start | bytes 2162688 | tf_op jit(solution)/shard_map/reduce_scatter | solution.py:149
  47.8 4.7 %copy-start.3 = (bf16[1,2048,768]{2,1,0:T(8,128)(2,1)S(1)}, bf16[1,2048,768]{2,1,0:T(8,128)(2,1)}, u32[]{:S(2)}) copy-start(bf16[1,2048,768]{2,1,0:T(8,128)(2,1)} %param.19) | copy-start | bytes 9437188
  47.8 4.7 %copy-start.5 = (bf16[512,2048]{1,0:T(8,128)(2,1)S(1)}, bf16[512,2048]{1,0:T(8,128)(2,1)}, u32[]{:S(2)}) copy-start(bf16[512,2048]{1,0:T(8,128)(2,1)} %all-gather.8.cloned.1.call-done) | copy-start | bytes 6291460
  90.5 1.9 copy-start.7
  90.5 1.9 copy-start.6
  90.5 2.5 copy-start.4
  96.1 155.6 %copy-start.2 = (bf16[128,256]{1,0:T(8,128)(2,1)S(1)}, bf16[128,256]{1,0:T(8,128)(2,1)}, u32[]{:S(2)}) copy-start(bf16[128,256]{1,0:T(8,128)(2,1)} %param.22) | copy-start | bytes 196612
  96.1 202.2 %reduce-scatter.5.cloned.1.call-start = ((), (), s32[]{:S(2)}) async-start(), calls=%async_computation.5 | async-start | bytes 1310720 | tf_op jit(solution)/shard_map/reduce_scatter | solution.py:169
  250.9 0.8 copy-start.1
Sparse Core Ops, SparseCore 0:
  9.8 37.8 all-gather.7
  49.6 35.1 all-gather.5
  96.2 138.5 reduce-scatter.2
  253.3 24.4 reduce-scatter.4

commit v2 on v1

--- a/solution.py
+++ b/solution.py
@@ -32,7 +32,133 @@
     return ((row <= col) if upper else (row >= col)).astype(F32)
 
 
-def mix_kernel(grad_in, out_proj, queries, log_decay, mix_out, start_out):
+def there(sp=None, tp=None):
+    where = {}
+    if sp is not None:
+        where["sp"] = sp
+    if tp is not None:
+        where["tp"] = tp
+    return where
+
+
+def greet(partners):
+    barrier = pltpu.get_barrier_semaphore()
+    for partner in partners:
+        pl.semaphore_signal(
+            barrier, inc=1, device_id=partner, device_id_type=pl.DeviceIdType.MESH
+        )
+    pl.semaphore_wait(barrier, len(partners))
+
+
+def send(src, dst, sems, slot, partner):
+    copy = pltpu.make_async_remote_copy(
+        src_ref=src,
+        dst_ref=dst,
+        send_sem=sems[0].at[slot],
+        recv_sem=sems[1].at[slot],
+        device_id=partner,
+        device_id_type=pl.DeviceIdType.MESH,
+    )
+    copy.start()
+    return copy
+
+
+def gather_kernel(n, own_a, own_b, weights, decays, all_a, all_b, all_w, all_d, *sems):
+    me, lane = lax.axis_index("sp"), lax.axis_index("tp")
+    core = lax.rem(lane, 2)
+    twin = there(tp=lane + 1 - 2 * core)
+    rows = own_a.shape[0]
+    half = rows // 2
+    peers = [there(sp=lax.rem(me + d, n)) for d in range(1, n)]
+    greet(peers + [twin])
+    far, near = sems[:2], sems[2:4]
+    copies = []
+    for t, (own, full) in enumerate([(weights, all_w), (decays, all_d)]):
+        for d, peer in enumerate(peers):
+            copies.append(send(own, full.at[me], far, t * (n - 1) + d, peer))
+    bulk = []
+    pieces = pl.ds(pl.multiple_of(core * half, half), half)
+    for t, (own, full) in enumerate([(own_a, all_a), (own_b, all_b)]):
+        for d, peer in enumerate(peers):
+            at = pl.ds(pl.multiple_of(me * rows + core * half, half), half)
+            bulk.append(send(own.at[pieces], full.at[at], far, (t + 2) * (n - 1) + d, peer))
+    here = pl.ds(pl.multiple_of(me * rows, rows), rows)
+    all_a[here, :] = own_a[...]
+    all_b[here, :] = own_b[...]
+    all_w[me] = weights[...]
+    all_d[me] = decays[...]
+    for t, full in enumerate([all_a, all_b]):
+        for d in range(n - 1):
+            slot = t * (n - 1) + d
+            bulk[slot].wait_recv()
+            source = lax.rem(me + n - 1 - d, n)
+            at = pl.ds(pl.multiple_of(source * rows + core * half, half), half)
+            copies.append(send(full.at[at], full.at[at], near, slot, twin))
+    for copy in bulk:
+        copy.wait_send()
+    for copy in copies:
+        copy.wait()
+
+
+def sum_kernel(n, slots, cot, out, got_a, sum_a, got_b, sum_b, got_c, *sems):
+    me, lane = lax.axis_index("sp"), lax.axis_index("tp")
+    core = lax.rem(lane, 2)
+    z = lax.div(lane, 2)
+    half = got_a.shape[1]
+    depth = got_c.shape[0] + 1
+    piece = half // depth
+    rows = 2 * half
+    twin = there(tp=lane + 1 - 2 * core)
+    peers = [there(sp=lax.rem(me + d, n)) for d in range(1, n)]
+    along = [lax.rem(z + d, depth) for d in range(1, depth)]
+    lanes = [there(tp=2 * other + core) for other in along]
+    greet(peers + lanes + [twin])
+    a, b, c, d_, e = (sems[2 * i : 2 * i + 2] for i in range(5))
+
+    def rows_at(start, size):
+        return pl.ds(pl.multiple_of(start, size), size)
+
+    first = [
+        send(slots.at[rows_at(k * rows + (1 - core) * half, half)], got_a.at[k], a, k, twin)
+        for k in range(n)
+    ]
+    for k in range(n):
+        first[k].wait_recv()
+        mine = slots[rows_at(k * rows + core * half, half), :].astype(F32)
+        sum_a[k] = (mine + got_a[k].astype(F32)).astype(BF16)
+    second = [
+        send(sum_a.at[lax.rem(me + d, n)], got_b.at[d - 1], b, d - 1, peers[d - 1])
+        for d in range(1, n)
+    ]
+    total = sum_a[me].astype(F32)
+    for d in range(n - 1):
+        second[d].wait_recv()
+        total = total + got_b[d].astype(F32)
+    sum_b[...] = total.astype(BF16)
+    third = [
+        send(sum_b.at[rows_at(along[d] * piece, piece)], got_c.at[d], c, d, lanes[d])
+        for d in range(depth - 1)
+    ]
+    mine = rows_at(core * half + z * piece, piece)
+    total = cot[mine, :].astype(F32) + sum_b[rows_at(z * piece, piece), :].astype(F32)
+    for d in range(depth - 1):
+        third[d].wait_recv()
+        total = total + got_c[d].astype(F32)
+    out[mine, :] = total.astype(BF16)
+    fourth = [send(out.at[mine], out.at[mine], d_, d, lanes[d]) for d in range(depth - 1)]
+    for copy in fourth:
+        copy.wait_recv()
+    whole = rows_at(core * half, half)
+    fifth = send(out.at[whole], out.at[whole], e, 0, twin)
+    fifth.wait()
+    for copy in first + second + third + fourth:
+        copy.wait_send()
+
+
+def mix_kernel(n, grad_in, out_proj, queries, log_decay, mix_out, starts, *sems):
+    me = lax.axis_index("sp")
+    peers = [there(sp=lax.rem(me + d, n)) for d in range(1, n)]
+    greet(peers)
     mix = dot(grad_in[...], out_proj[...], NT, None)
     mix_out[...] = mix
     rows, channels = queries.shape
@@ -43,15 +169,52 @@
     for h in range(heads):
         keyed = slice(h * DK, (h + 1) * DK)
         carry = None
-        for n in reversed(range(rows // SPAN)):
-            at = slice(n * SPAN, (n + 1) * SPAN)
+        for n_ in reversed(range(rows // SPAN)):
+            at = slice(n_ * SPAN, (n_ + 1) * SPAN)
             decay = log_decay[at, keyed]
             qd = queries[at, keyed].astype(F32) * jnp.exp(dot(lower, decay, NN))
             local = DK**-0.5 * dot(qd, mix[at, h * wide : (h + 1) * wide], TN)
             if carry is not None:
                 local = local + jnp.exp(dot(decay, ones, TN)) * carry
             carry = local
-        start_out[keyed, :] = carry
+        starts[me, keyed, :] = carry
+    copies = [send(starts.at[me], starts.at[me], sems, d, peers[d]) for d in range(n - 1)]
+    for copy in copies:
+        copy.wait()
+
+
+def weight_kernel(inputs, routed, hidden, d_gate, d_upper, gate_o, up_o, down_o):
+    gate_o[0] = dot(inputs[...], d_gate[...], TN, None).astype(BF16)
+    up_o[0] = dot(inputs[...], d_upper[...], TN, None).astype(BF16)
+    down_o[0] = dot(hidden[...], routed[...], TN, None).astype(BF16)
+
+
+def weight_grads(inputs, routed, hidden, d_gate, d_upper):
+    slots, width = inputs.shape
+    units = hidden.shape[1]
+    tile = width // 8
+    moving = pl.BlockSpec((slots, tile), lambda i: (0, i))
+    still = pl.BlockSpec((slots, units), lambda i: (0, 0))
+    return pl.pallas_call(
+        weight_kernel,
+        grid=(width // tile,),
+        out_shape=[
+            jax.ShapeDtypeStruct((1, width, units), BF16),
+            jax.ShapeDtypeStruct((1, width, units), BF16),
+            jax.ShapeDtypeStruct((1, units, width), BF16),
+        ],
+        in_specs=[moving, moving, still, still, still],
+        out_specs=[
+            pl.BlockSpec((1, tile, units), lambda i: (0, i, 0)),
+            pl.BlockSpec((1, tile, units), lambda i: (0, i, 0)),
+            pl.BlockSpec((1, units, tile), lambda i: (0, 0, i)),
+        ],
+        cost_estimate=pl.CostEstimate(
+            flops=6 * slots * width * units,
+            bytes_accessed=6 * width * units,
+            transcendentals=0,
+        ),
+    )(inputs, routed, hidden, d_gate, d_upper)
 
 
 def finish_kernel(queries, keys, values, log_decay, mix, state, after, dq_o, dk_o, dv_o, dl_o):
@@ -93,13 +256,18 @@
                 g_end = DK**-0.5 * dot(qd, g, TN) + e_last * g_end
 
 
-def call(kernel, outs, *args):
+def call(kernel, outs, *args, scratch=(), sems=(), ident=None):
+    semaphores = [pltpu.SemaphoreType.DMA((count,)) for count in sems for _ in range(2)]
     return pl.pallas_call(
         kernel,
         out_shape=[jax.ShapeDtypeStruct(s, d) for s, d in outs],
         in_specs=[pl.BlockSpec(memory_space=pltpu.VMEM)] * len(args),
         out_specs=[pl.BlockSpec(memory_space=pltpu.VMEM)] * len(outs),
+        scratch_shapes=[pltpu.VMEM(s, BF16) for s in scratch] + semaphores,
         cost_estimate=pl.CostEstimate(flops=2 * 10**8, bytes_accessed=10**6, transcendentals=0),
+        compiler_params=pltpu.CompilerParams(
+            collective_id=ident, has_side_effects=ident is not None
+        ),
     )(*args)
 
 
@@ -123,17 +291,26 @@
     groups = lax.axis_size("sp")
     lanes = lax.axis_size("tp")
     me = lax.axis_index("sp")
-    lane = lax.axis_index("tp")
-    inputs = lax.all_gather(moe_input, "sp", axis=0, tiled=True)
-    cots = lax.all_gather(cotangent, "sp", axis=0, tiled=True)
     named = route_expert[:, :, None] == jnp.arange(groups, dtype=jnp.int32)
     weights = jnp.sum(jnp.where(named, route_weight[:, :, None], 0.0), axis=1).T
-    small = lax.all_gather(
-        jnp.concatenate([weights.reshape(-1), jnp.sum(log_decay, axis=0)]), "sp"
-    )
-    weights_all = small[:, : groups * tok_rows].reshape(groups, groups, tok_rows)
+    decay_sum = jnp.sum(log_decay, axis=0, keepdims=True)
+    inputs, cots, weights_all, decays = call(
+        functools.partial(gather_kernel, groups),
+        [
+            ((groups * tok_rows, width), BF16),
+            ((groups * tok_rows, width), BF16),
+            ((groups, groups, tok_rows), F32),
+            ((groups, 1, log_decay.shape[1]), F32),
+        ],
+        moe_input,
+        cotangent,
+        weights,
+        decay_sum,
+        sems=(4 * (groups - 1), 2 * (groups - 1)),
+        ident=1,
+    )
     mine = lax.dynamic_index_in_dim(weights_all, me, 1, keepdims=False).reshape(-1, 1)
-    decays = small[:, groups * tok_rows :]
+    decays = decays[:, 0]
 
     gate_weight, up_weight, down_weight = w_gate[0], w_up[0], w_down[0]
     gate = jnp.dot(inputs, gate_weight, preferred_element_type=F32)
@@ -146,26 +323,35 @@
     d_upper = (d_hidden * active).astype(BF16)
     d_gate = (d_hidden * upper * sigmoid_gate * (1.0 + gate * (1.0 - sigmoid_gate))).astype(BF16)
     slots = (dot(d_gate, gate_weight, NT, None) + dot(d_upper, up_weight, NT, None)).astype(BF16)
-    part = lax.psum_scatter(slots, ("sp", "tp"), scatter_dimension=0, tiled=True)
-    grad_down = dot(hidden, routed, TN, None).astype(BF16)
-    grad_gate = dot(inputs, d_gate, TN, None).astype(BF16)
-    grad_up = dot(inputs, d_upper, TN, None).astype(BF16)
-
-    share = tok_rows // lanes
-    own = lax.dynamic_slice_in_dim(cotangent, lane * share, share, 0)
-    part = (own.astype(F32) + part.astype(F32)).astype(BF16)
-    grad_in = lax.all_gather(part, "tp", axis=0, tiled=True)
+    half, depth = tok_rows // 2, lanes // 2
+    (grad_in,) = call(
+        functools.partial(sum_kernel, groups),
+        [((tok_rows, width), BF16)],
+        slots,
+        cotangent,
+        scratch=[
+            (groups, half, width),
+            (groups, half, width),
+            (groups - 1, half, width),
+            (half, width),
+            (depth - 1, half // depth, width),
+        ],
+        sems=(groups, groups - 1, depth - 1, depth - 1, 1),
+        ident=2,
+    )
+    grad_gate, grad_up, grad_down = weight_grads(inputs, routed, hidden, d_gate, d_upper)
 
     channels, wide = queries.shape[1], span_state.shape[2]
-    mix, start = call(
-        mix_kernel,
-        [((tok_rows, values.shape[1]), F32), ((channels, wide), F32)],
+    mix, starts = call(
+        functools.partial(mix_kernel, groups),
+        [((tok_rows, values.shape[1]), F32), ((groups, channels, wide), F32)],
         grad_in,
         out_proj,
         queries,
         log_decay,
-    )
-    starts = lax.all_gather(start, "sp")
+        sems=(groups - 1,),
+        ident=3,
+    )
     grad_proj = lax.psum_scatter(
         dot(grad_in, saved_out, TN, None).astype(BF16), "sp", scatter_dimension=0, tiled=True
     ).astype(F32)
@@ -191,9 +377,9 @@
         after,
     )
     return (
-        grad_gate[None],
-        grad_up[None],
-        grad_down[None],
+        grad_gate,
+        grad_up,
+        grad_down,
         grad_proj,
         grad_queries,
         grad_keys,

time: 307 us -> 144 us (0.47)
  waiting for transfers between devices: 197 us -> 0.02 us
  Pallas kernels: 9.56 us -> 96.5 us
  blocking collectives: 33.2 us -> 0 us
  matrix products: 36.7 us -> 21.9 us
  local copies, waits for them, and re-layouts: 10.9 us -> 1.71 us
  other arithmetic: 5.19 us -> 8.64 us
    reduce_scatter x1 -> x0, waiting for transfers between devices: 139 us -> none  [on_device(): lax.psum_scatter(slots, ('sp', 'tp'), scatter_dimension=0, tiled=True)]
    pallas_call x2 -> x4, Pallas kernels: 9.56 us -> 86.1 us  [call(): pl.pallas_call(kernel, out_shape=[jax.ShapeDtypeStruct(s, d) for s, d in...]
    all_gather x2 -> x0, waiting for transfers between devices: 57.1 us -> none  [the longest x1 29.3 us: on_device(): cots = lax.all_gather(cotangent, 'sp', axis=0, tiled=True)]
    all_gather x3 -> x0, blocking collectives: 33.2 us -> none  [the longest x1 15.1 us: on_device(): grad_in = lax.all_gather(part, 'tp', axis=0, tiled=True)]
    dot_general x7 -> x4, matrix products: 29 us -> 13.4 us  [dot(): lax.dot_general(a, b, ((dims[0], dims[1]), ((), ())), precision=precision...]
    pallas_call x0 -> x1, Pallas kernels: none -> 10.3 us  [weight_grads(): pl.pallas_call(weight_kernel, grid=(width // tile,), out_shape=[jax.Shape...]
    unnamed x20 -> x18, local copies, waits for them, and re-layouts: 10.8 us -> 1 us
  transfers between devices with their start and end apart: 4 -> 1, of which waited for: 3 -> 0; matrix products, arithmetic and copies ran while one was open for 12% -> 1% of each run, Pallas kernels for 3% -> 20%
where the time goes in v2:
time: 144 us; the launch traced here: 143 us
  Pallas kernels  96.5 us (67%)
  matrix products  21.9 us (15%)
  between operations  14.2 us (10%)
  other arithmetic  8.64 us (6%)
  local copies, waits for them, and re-layouts  1.71 us (1%)
    pallas_call x4, Pallas kernels, call(): pl.pallas_call(kernel, out_shape=[jax.ShapeDtypeStruct(s, d) for s, d in...  86.1 us
    dot_general x4, matrix products, dot(): lax.dot_general(a, b, ((dims[0], dims[1]), ((), ())), precision=precision...  13.4 us
    pallas_call x1, Pallas kernels, weight_grads(): pl.pallas_call(weight_kernel, grid=(width // tile,), out_shape=[jax.Shape...  10.3 us
    dot_general x1, matrix products, on_device(): gate = jnp.dot(inputs, gate_weight, preferred_element_type=F32)  5.61 us
    dot_general x1, matrix products, on_device(): upper = jnp.dot(inputs, up_weight, preferred_element_type=F32)  2.94 us
  transfers between devices with their start and end apart: 1, of which 0 were waited for; matrix products, arithmetic and copies ran while one was open for 1% of the time, Pallas kernels for 20%

profile of v2, /device:TPU:0, one launch (start us, length us, event | category | flops | bytes accessed | tf_op | source)
XLA Modules:
  0.0 142.9 jit_solution(11552927922912678426)
XLA Ops:
  7.2 0.0 copy-start
  7.2 0.0 reduce-scatter.2.cloned.1.call-start
  7.2 1.4 %select_reduce_fusion = f32[128,4]{0,1:T(4,128)} fusion(f32[128,2]{0,1:T(2,128)} %param.17, s32[128,2]{0,1:T(2,128)} %param.16), kind=kLoop, calls=%fused_computation.20 | loop fusion | flops 2560 | bytes 4096 | tf_op jit(solution)/shard_map/reduce_sum | solution.py:295
  8.7 1.4 reduce_sum.37
  10.0 32.5 %shard_map.197 = (bf16[512,2048]{1,0:T(8,128)(2,1)}, bf16[512,2048]{1,0:T(8,128)(2,1)}, f32[4,4,128]{2,1,0:T(4,128)}, f32[4,1,128]{2,1,0:T(1,128)}) custom-call(bf16[128,2048]{1,0:T(8,128)(2,1)} %own_a.1, bf16[128,2048]{1,0:T(8,128)(2,1)} %cot.1, f32[4,128]{1,0:T(4,128)} %bitcast.28, f32[1,128]{1,0:T(1,128)} %bitcast.30), custom_call_target="tpu_custom_call" | custom-call | flops 200000000 | bytes 1000000 | tf_op jit(solution)/shard_map/pallas_call | solution.py:261
  42.6 5.6 %fusion.8 = f32[512,768]{1,0:T(8,128)} fusion(bf16[512,2048]{1,0:T(8,128)(2,1)} %get-tuple-element.21.inputs, bf16[1,2048,768]{2,1,0:T(8,128)(2,1)} %param.18), kind=kOutput, calls=%fused_computation.10 | convolution fusion | flops 1610612736 | bytes 6815744 | tf_op jit(solution)/shard_map/dot_general | solution.py:316
  48.2 2.9 %fusion.4 = f32[512,768]{1,0:T(8,128)} fusion(bf16[512,2048]{1,0:T(8,128)(2,1)S(1)} %copy-done.6, bf16[1,2048,768]{2,1,0:T(8,128)(2,1)S(1)} %copy-done), kind=kOutput, calls=%fused_computation.6 | convolution fusion | flops 1610612736 | bytes 6815744 | tf_op jit(solution)/shard_map/dot_general | solution.py:317
  51.1 0.7 constant_dynamic-slice_fusion
  51.8 2.1 %multiply_convert_fusion.routed = bf16[512,2048]{1,0:T(8,128)(2,1)S(1)} fusion(bf16[512,2048]{1,0:T(8,128)(2,1)} %get-tuple-element.23, f32[512]{0:T(512)S(1)} %bitcast.29), kind=kLoop, calls=%fused_computation.1 | loop fusion | flops 3145728 | bytes 4196352 | tf_op jit(solution)/shard_map/convert_element_type | solution.py:318
  54.0 0.4 copy-done.4
  54.3 5.9 %multiply_convert_fusion.1 = (bf16[512,768]{1,0:T(8,128)(2,1)S(1)}, bf16[512,768]{1,0:T(8,128)(2,1)S(1)}, bf16[512,768]{1,0:T(8,128)(2,1)}) fusion(f32[512,768]{1,0:T(8,128)} %fusion.8, f32[512,768]{1,0:T(8,128)} %fusion.4, bf16[512,2048]{1,0:T(8,128)(2,1)S(1)} %multiply_convert_fusion.routed, bf16[1,768,2048]{2,1,0:T(8,128)(2,1)S(1)} %copy-done.4), kind=kOutput, calls=%fused_computation.13 | convolution fusion | flops 1616510976 | bytes 10747904 | tf_op jit(solution)/shard_map/dot_general | solution.py:19
  60.3 1.8 %fusion.2 = f32[512,2048]{1,0:T(8,128)S(1)} fusion(bf16[512,768]{1,0:T(8,128)(2,1)S(1)} %get-tuple-element.34.d_upper, bf16[1,2048,768]{2,1,0:T(8,128)(2,1)S(1)} %copy-done), kind=kOutput, calls=%fused_computation.4 | convolution fusion | flops 1610612736 | bytes 8126464 | tf_op jit(solution)/shard_map/dot_general | solution.py:19
  62.1 0.6 copy-done.5
  62.7 3.1 %add_convert_fusion.slots = bf16[512,2048]{1,0:T(8,128)(2,1)} fusion(f32[512,2048]{1,0:T(8,128)S(1)} %fusion.2, bf16[512,768]{1,0:T(8,128)(2,1)S(1)} %get-tuple-element.35.d_gate, bf16[1,2048,768]{2,1,0:T(8,128)(2,1)S(1)} %copy-done.5), kind=kOutput, calls=%fused_computation | convolution fusion | flops 1612709888 | bytes 10223616 | tf_op jit(solution)/shard_map/dot_general | solution.py:19
  65.9 35.6 %shard_map.199.grad_in = bf16[128,2048]{1,0:T(8,128)(2,1)} custom-call(bf16[512,2048]{1,0:T(8,128)(2,1)} %add_convert_fusion.slots, bf16[128,2048]{1,0:T(8,128)(2,1)} %cot.1), custom_call_target="tpu_custom_call" | custom-call | flops 200000000 | bytes 1000000 | tf_op jit(solution)/shard_map/pallas_call | solution.py:261
  101.5 2.5 %convolution_convert_fusion = bf16[2048,256]{1,0:T(8,128)(2,1)} fusion(bf16[128,2048]{1,0:T(8,128)(2,1)} %shard_map.199.grad_in, bf16[128,256]{1,0:T(8,128)(2,1)S(1)} %copy-done.2), kind=kOutput, calls=%fused_computation.12 | convolution fusion | flops 134742016 | bytes 1638400 | tf_op jit(solution)/shard_map/dot_general | solution.py:19
  104.0 0.0 reduce-scatter.2.cloned.1.call-update
  104.0 12.6 %shard_map.200 = (f32[128,256]{1,0:T(8,128)}, f32[4,128,128]{2,1,0:T(8,128)}) custom-call(bf16[128,2048]{1,0:T(8,128)(2,1)} %shard_map.199.grad_in, bf16[256,2048]{1,0:T(8,128)(2,1)} %out_proj.1, bf16[128,128]{1,0:T(8,128)(2,1)} %queries.3, f32[128,128]{1,0:T(8,128)} %log_decay.3), custom_call_target="tpu_custom_call" | custom-call | flops 200000000 | bytes 1000000 | tf_op jit(solution)/shard_map/pallas_call | solution.py:261
  116.7 0.1 multiply_reduce_fusion.1
  116.8 0.1 exponential_select_fusion
  116.8 1.7 %multiply_reduce_fusion.after = f32[128,128]{1,0:T(8,128)} fusion(f32[4,128,128]{2,1,0:T(8,128)} %get-tuple-element.29, f32[4,128]{1,0:T(4,128)S(1)} %exponential_select_fusion), kind=kLoop, calls=%fused_computation.18 | loop fusion | flops 114688 | bytes 329728 | tf_op jit(solution)/shard_map/reduce_sum | solution.py:362
  118.6 5.4 %shard_map.201 = (bf16[128,128]{1,0:T(8,128)(2,1)}, bf16[128,128]{1,0:T(8,128)(2,1)}, bf16[128,256]{1,0:T(8,128)(2,1)}, f32[128,128]{1,0:T(8,128)}) custom-call(bf16[128,128]{1,0:T(8,128)(2,1)} %queries.3, bf16[128,128]{1,0:T(8,128)(2,1)} %keys.1, bf16[128,256]{1,0:T(8,128)(2,1)} %values.1, f32[128,128]{1,0:T(8,128)} %log_decay.3, ...), custom_call_target="tpu_custom_call" | custom-call | flops 200000000 | bytes 1000000 | tf_op jit(solution)/shard_map/pallas_call | solution.py:261
  124.0 10.3 %shard_map.198 = (bf16[1,2048,768]{2,1,0:T(8,128)(2,1)}, bf16[1,2048,768]{2,1,0:T(8,128)(2,1)}, bf16[1,768,2048]{2,1,0:T(8,128)(2,1)}) custom-call(bf16[512,2048]{1,0:T(8,128)(2,1)} %get-tuple-element.21.inputs, bf16[512,2048]{1,0:T(8,128)(2,1)} %copy-done.1, bf16[512,768]{1,0:T(8,128)(2,1)} %get-tuple-element.36.hidden, bf16[512,768]{1,0:T(8,128)(2,1)} %copy-done.7, ...), custom_call_target="tpu_custom_call" | custom-call | flops 4831838208 | bytes 9437184 | tf_op jit(solution)/shard_map/pallas_call | solution.py:198
  134.3 1.8 %convert_element_type.38 = f32[512,256]{1,0:T(8,128)} convert(bf16[512,256]{1,0:T(8,128)(2,1)} %reduce-scatter.2.cloned.1.call-done) | non-fusion elementwise | flops 131072 | bytes 786432 | tf_op jit(solution)/shard_map/convert_element_type | solution.py:357
  (18 shorter events, 0.0 us)
Async XLA Ops:
  7.2 41.0 %copy-start = (bf16[1,2048,768]{2,1,0:T(8,128)(2,1)S(1)}, bf16[1,2048,768]{2,1,0:T(8,128)(2,1)}, u32[]{:S(2)}) copy-start(bf16[1,2048,768]{2,1,0:T(8,128)(2,1)} %param.19) | copy-start | bytes 9437188
  7.2 127.1 %reduce-scatter.2.cloned.1.call-start = ((), (), s32[]{:S(2)}) async-start(), calls=%async_computation.1 | async-start | bytes 1310720 | tf_op jit(solution)/shard_map/reduce_scatter | solution.py:355
  42.6 5.6 %copy-start.6 = (bf16[512,2048]{1,0:T(8,128)(2,1)S(1)}, bf16[512,2048]{1,0:T(8,128)(2,1)}, u32[]{:S(2)}) copy-start(bf16[512,2048]{1,0:T(8,128)(2,1)} %get-tuple-element.21.inputs) | copy-start | bytes 6291460
  51.8 2.5 %copy-start.4 = (bf16[1,768,2048]{2,1,0:T(8,128)(2,1)S(1)}, bf16[1,768,2048]{2,1,0:T(8,128)(2,1)}, u32[]{:S(2)}) copy-start(bf16[1,768,2048]{2,1,0:T(8,128)(2,1)} %param.20) | copy-start | bytes 9437188
  54.3 5.9 %copy-start.1 = (bf16[512,2048]{1,0:T(8,128)(2,1)}, bf16[512,2048]{1,0:T(8,128)(2,1)S(1)}, u32[]{:S(2)}) copy-start(bf16[512,2048]{1,0:T(8,128)(2,1)S(1)} %multiply_convert_fusion.routed) | copy-start | bytes 6291460
  60.3 1.8 %copy-start.8 = (bf16[512,768]{1,0:T(8,128)(2,1)}, bf16[512,768]{1,0:T(8,128)(2,1)S(1)}, u32[]{:S(2)}) copy-start(bf16[512,768]{1,0:T(8,128)(2,1)S(1)} %get-tuple-element.34.d_upper) | copy-start | bytes 2359300
  60.3 1.9 %copy-start.7 = (bf16[512,768]{1,0:T(8,128)(2,1)}, bf16[512,768]{1,0:T(8,128)(2,1)S(1)}, u32[]{:S(2)}) copy-start(bf16[512,768]{1,0:T(8,128)(2,1)S(1)} %get-tuple-element.35.d_gate) | copy-start | bytes 2359300
  60.3 2.5 %copy-start.5 = (bf16[1,2048,768]{2,1,0:T(8,128)(2,1)S(1)}, bf16[1,2048,768]{2,1,0:T(8,128)(2,1)}, u32[]{:S(2)}) copy-start(bf16[1,2048,768]{2,1,0:T(8,128)(2,1)} %param.18) | copy-start | bytes 9437188
  65.9 35.6 %copy-start.2 = (bf16[128,256]{1,0:T(8,128)(2,1)S(1)}, bf16[128,256]{1,0:T(8,128)(2,1)}, u32[]{:S(2)}) copy-start(bf16[128,256]{1,0:T(8,128)(2,1)} %param.22) | copy-start | bytes 196612
  101.5 15.2 %copy-start.3 = (f32[4,1,128]{2,1,0:T(1,128)S(1)}, f32[4,1,128]{2,1,0:T(1,128)}, u32[]{:S(2)}) copy-start(f32[4,1,128]{2,1,0:T(1,128)} %get-tuple-element.28) | copy-start | bytes 6148
Sparse Core Ops, SparseCore 0:
  104.1 29.5 reduce-scatter.1
